TPU v7x, 32 devices: a whole 2x2x4 slice. The times are simulated.
32 devices in a mesh: ep: 8 (over z, x), tp: 4 (over y, core).
Axes of the slice: x: 2, y: 2, z: 4, core: 2. Of those that a mesh axis runs over, the one named last changes fastest.
Arguments:
- query_latent: bfloat16 [1024, 512], P('ep'), may hold values from -6 to 6
- key_latent: bfloat16 [1024, 256], P('ep'), may hold values from -6 to 6
- rope_key: bfloat16 [1024, 64], P('ep'), may hold values from -500 to 500
- query_gain: float32 [512], replicated, may hold values from 0.1 to 1.9
- key_gain: float32 [256], replicated, may hold values from 0.1 to 1.9
- w_query: bfloat16 [512, 1024], P(None, 'tp'), may hold values from -0.25 to 0.25
- w_query_rope: bfloat16 [512, 512], P(None, 'tp'), may hold values from -0.25 to 0.25
- w_key: bfloat16 [256, 1024], P(None, 'tp'), may hold values from -0.375 to 0.375
- w_value: bfloat16 [256, 1024], P(None, 'tp'), may hold values from -0.375 to 0.375
- w_out: bfloat16 [1024, 2048], P('tp'), may hold values from -1.796875 to 1.796875
- tokens_b: bfloat16 [4096, 2048], P('ep'), may hold values from -6 to 6
- ffn_gain: float32 [2048], replicated, may hold values from 0.1 to 1.9
- route_expert: int32 [4096, 2], P('ep'), may hold values from 0 to 7, as said below
- route_weight: float32 [4096, 2], P('ep'), may hold values from 0.2 to 1
- w_gate: bfloat16 [8, 2048, 1024], P('ep', None, 'tp'), may hold values from -0.125 to 0.125
- w_up: bfloat16 [8, 2048, 1024], P('ep', None, 'tp'), may hold values from -0.125 to 0.125
- w_down: bfloat16 [8, 1024, 2048], P('ep', 'tp'), may hold values from -0.1875 to 0.1875
Outputs:
- mixer_out: bfloat16 [1024, 2048], P(('ep', 'tp'))
- moe_out: bfloat16 [4096, 2048], P('ep', 'tp')
Inputs may be any that keep to these rules, and one draw needn't show every extreme that they name: `route_expert`: expert e belongs to group e // 2. A row's 2 experts differ and lie in one group. Among the rows of one device along ep, every group is named by exactly 128 rows and every expert is named exactly 128 times.
All inputs are finite; a program needn't handle non-finite values.
Results may differ from a plain program's by a relative error of at most 0.013.
The roundings to bfloat16 on the way count: a program that leaves them out, or rounds other values in their place, can miss the bound.
Values may be sent and summed in bfloat16 or wider, within the bound.
A program may use at most 64 MiB of HBM per device.

v0:
```python
import math
import jax
import jax.numpy as jnp
from jax import lax
from jax.sharding import PartitionSpec as P

NOPE = 128
ROPE = 64
VDIM = 128
GRID_W = 64
TOPK = 2
epsilon = 1e-06
rotary_base = 10000.0
neg_large = -1e30


def rms_scale(values_in, gain):
    widened = values_in.astype(jnp.float32)
    normed = widened * lax.rsqrt(jnp.mean(widened * widened, axis=-1, keepdims=True) + epsilon)
    return (normed * gain).astype(jnp.bfloat16)


def rotary_tables(positions):
    half_width = ROPE // 2
    inverse = rotary_base ** (-jnp.arange(0, half_width, 2, dtype=jnp.float32) / half_width)
    grid_row = (positions // GRID_W).astype(jnp.float32)
    grid_col = (positions % GRID_W).astype(jnp.float32)
    angle = jnp.concatenate([grid_row[:, None] * inverse, grid_col[:, None] * inverse], axis=-1)
    return (jnp.cos(angle), jnp.sin(angle))


def rotate(values_in, cosine, sine):
    even_part = values_in[..., 0::2]
    odd_part = values_in[..., 1::2]
    turned = jnp.stack(
        [even_part * cosine - odd_part * sine, even_part * sine + odd_part * cosine], axis=-1
    )
    return turned.reshape(values_in.shape)


def fold_blocks(carry, members, step_fn):
    piece_rows = members[0].shape[0]
    block_rows = math.gcd(piece_rows, 1024)
    if block_rows == piece_rows:
        return step_fn(carry, members)
    stacked = tuple(
        (
            member.reshape((piece_rows // block_rows, block_rows) + member.shape[1:])
            for member in members
        )
    )

    def scan_step(inner_carry, blocks):
        return (step_fn(inner_carry, blocks), None)

    result, unused = lax.scan(scan_step, carry, stacked)
    return result


def mixer_half(
    query_latent,
    key_latent,
    rope_key,
    query_gain,
    key_gain,
    w_query,
    w_query_rope,
    w_key,
    w_value,
    w_out,
):
    tok_rows = query_latent.shape[0]
    local_heads = w_query.shape[1] // NOPE
    positions = lax.axis_index("ep") * tok_rows + jnp.arange(tok_rows, dtype=jnp.int32)
    cosine, sine = rotary_tables(positions)
    query_normed = rms_scale(query_latent, query_gain)
    query_nope = jnp.dot(query_normed, w_query, preferred_element_type=jnp.float32).astype(
        jnp.bfloat16
    )
    query_nope = query_nope.reshape(tok_rows, local_heads, NOPE)
    query_rot = jnp.dot(query_normed, w_query_rope, preferred_element_type=jnp.float32)
    query_rot = rotate(
        query_rot.reshape(tok_rows, local_heads, ROPE), cosine[:, None, :], sine[:, None, :]
    )
    query_rot = query_rot.astype(jnp.bfloat16)
    key_rot = rotate(rope_key.astype(jnp.float32), cosine, sine).astype(jnp.bfloat16)
    score_scale = (NOPE + ROPE) ** (-0.5)

    def expand(latent_rows):
        latent_count = latent_rows.shape[0]
        key_normed = rms_scale(latent_rows, key_gain)
        key_nope = jnp.dot(key_normed, w_key, preferred_element_type=jnp.float32).astype(
            jnp.bfloat16
        )
        value_rows = jnp.dot(key_normed, w_value, preferred_element_type=jnp.float32).astype(
            jnp.bfloat16
        )
        return (
            key_nope.reshape(latent_count, local_heads, NOPE),
            value_rows.reshape(latent_count, local_heads, VDIM),
        )

    def attend_block(carry, key_nope, value_rows, key_turn):
        run_max, run_total, run_acc = carry
        scores = jnp.einsum(
            "qhd,khd->hqk", query_nope, key_nope, preferred_element_type=jnp.float32
        )
        scores = scores + jnp.einsum(
            "qhd,kd->hqk", query_rot, key_turn, preferred_element_type=jnp.float32
        )
        scores = scores * score_scale
        new_max = jnp.maximum(run_max, jnp.max(scores, axis=-1))
        correction = jnp.exp(run_max - new_max)
        weights = jnp.exp(scores - new_max[..., None])
        new_total = run_total * correction + jnp.sum(weights, axis=-1)
        added = jnp.einsum(
            "hqk,khd->qhd",
            weights.astype(jnp.bfloat16),
            value_rows,
            preferred_element_type=jnp.float32,
        )
        new_acc = run_acc * jnp.transpose(correction)[..., None] + added
        return (new_max, new_total, new_acc)

    def step_latent(carry, blocks):
        key_nope, value_rows = expand(blocks[0])
        return attend_block(carry, key_nope, value_rows, blocks[1])

    initial = (
        jnp.full((local_heads, tok_rows), neg_large, jnp.float32),
        jnp.zeros((local_heads, tok_rows), jnp.float32),
        jnp.zeros((tok_rows, local_heads, VDIM), jnp.float32),
    )
    final = fold_blocks(
        initial,
        (
            lax.all_gather(key_latent, "ep", axis=0, tiled=True),
            lax.all_gather(key_rot, "ep", axis=0, tiled=True),
        ),
        step_latent,
    )
    run_max, run_total, run_acc = final
    heads_out = (run_acc / jnp.transpose(run_total)[..., None]).astype(jnp.bfloat16)
    heads_out = heads_out.reshape(tok_rows, local_heads * VDIM)
    return lax.psum_scatter(
        jnp.dot(heads_out, w_out, preferred_element_type=jnp.float32).astype(jnp.bfloat16),
        "tp",
        scatter_dimension=0,
        tiled=True,
    )


def expert_half(tokens_b, ffn_gain, route_expert, route_weight, w_gate, w_up, w_down):
    tok_rows = tokens_b.shape[0]
    expert_count = lax.axis_size("ep")
    capacity = TOPK * tok_rows // expert_count
    normed = rms_scale(tokens_b, ffn_gain)
    copies = route_expert.reshape(tok_rows * TOPK)
    chosen = (copies[:, None] == jnp.arange(expert_count, dtype=jnp.int32)[None, :]).astype(
        jnp.int32
    )
    earlier = jnp.cumsum(chosen, axis=0) - chosen
    slot_index = jnp.sum(earlier * chosen, axis=1)
    target = copies * capacity + slot_index
    source_row = (
        jnp.zeros((expert_count * capacity,), jnp.int32)
        .at[target]
        .set(jnp.arange(tok_rows * TOPK, dtype=jnp.int32) // TOPK)
    )
    outgoing = jnp.take(normed, source_row, axis=0)
    share_cols = outgoing.shape[1] // lax.axis_size("tp")
    own_cols = lax.dynamic_slice_in_dim(outgoing, lax.axis_index("tp") * share_cols, share_cols, 1)
    arrived = lax.all_to_all(own_cols, "ep", split_axis=0, concat_axis=0, tiled=True)
    member = lax.all_gather(arrived, "tp", axis=1, tiled=True)
    gate_rows = w_gate[0]
    up_rows = w_up[0]
    gate_act = jnp.dot(member, gate_rows, preferred_element_type=jnp.float32)
    up_act = jnp.dot(member, up_rows, preferred_element_type=jnp.float32)
    hidden = (jax.nn.silu(gate_act) * up_act).astype(jnp.bfloat16)
    partial_term = jnp.dot(hidden, w_down[0], preferred_element_type=jnp.float32)
    shared = lax.psum_scatter(
        partial_term.astype(jnp.bfloat16), "tp", scatter_dimension=1, tiled=True
    )
    returned = lax.all_to_all(shared, "ep", split_axis=0, concat_axis=0, tiled=True)
    picked = (
        jnp.take(returned, target, axis=0)
        .astype(jnp.float32)
        .reshape(tok_rows, TOPK, returned.shape[1])
    )
    combined = jnp.sum(picked * route_weight[:, :, None], axis=1)
    return combined.astype(jnp.bfloat16)


def body(
    query_latent,
    key_latent,
    rope_key,
    query_gain,
    key_gain,
    w_query,
    w_query_rope,
    w_key,
    w_value,
    w_out,
    tokens_b,
    ffn_gain,
    route_expert,
    route_weight,
    w_gate,
    w_up,
    w_down,
):
    mixer_out = mixer_half(
        query_latent,
        key_latent,
        rope_key,
        query_gain,
        key_gain,
        w_query,
        w_query_rope,
        w_key,
        w_value,
        w_out,
    )
    moe_out = expert_half(tokens_b, ffn_gain, route_expert, route_weight, w_gate, w_up, w_down)
    return (mixer_out, moe_out)


def solution(mesh):
    in_specs = (
        P("ep", None),
        P("ep", None),
        P("ep", None),
        P(),
        P(),
        P(None, "tp"),
        P(None, "tp"),
        P(None, "tp"),
        P(None, "tp"),
        P("tp", None),
        P("ep", None),
        P(),
        P("ep", None),
        P("ep", None),
        P("ep", None, "tp"),
        P("ep", None, "tp"),
        P("ep", "tp", None),
    )
    out_specs = (P(("ep", "tp"), None), P("ep", "tp"))
    return jax.shard_map(body, mesh=mesh, in_specs=in_specs, out_specs=out_specs, check_vma=False)
```

profile of v0, /device:TPU:0, one launch (start us, length us, event | category | flops | bytes accessed | tf_op | source)
XLA Modules:
  0.0 206.5 jit_solution(17284445992472675687)
XLA Ops:
  7.2 0.9 copy.40
  8.5 0.7 broadcast_multiply_fusion.2
  9.2 2.3 %reduce-window.6 = s32[8,8,128]{2,1,0:T(8,128)S(1)} reduce-window(s32[8,8,128]{2,1,0:T(8,128)S(1)} %fusion.43, s32[]{:T(128)} %constant.106.clone.1), window={size=1x1x128 pad=0_0x0_0x127_0}, to_apply=%region_5.6 | reduce-window | flops 1040384 | bytes 65540 | tf_op jit(solution)/shard_map/reduce-window
  11.5 0.3 slice_reduce_fusion
  12.4 4.3 %scatter_custom_fusion = s32[1024]{0:T(1024)S(1)} fusion(s32[1024]{0:T(1024)S(1)} %bitcast.101, s32[1024]{0:T(1024)S(1)} %add_select_fusion, s32[]{:T(128)} %constant.106.clone.1), kind=kCustom, calls=%fused_computation.95 | custom fusion | bytes 4100 | tf_op jit(solution)/shard_map/scatter | solution.py:168
  16.7 2.1 %fusion = f32[512]{0:T(512)S(1)} fusion(bf16[512,2048]{1,0:T(8,128)(2,1)} %param.27), kind=kLoop, calls=%fused_computation.5 | loop fusion | flops 3145216 | bytes 2099200 | tf_op jit(solution)/shard_map/reduce_sum | solution.py:19
  18.8 2.1 %fusion.2 = bf16[512,2048]{1,0:T(8,128)(2,1)S(1)} fusion(bf16[512,2048]{1,0:T(8,128)(2,1)} %param.27, f32[2048]{0:T(1024)} %param.28, f32[512]{0:T(512)S(1)} %add_rsqrt_fusion.1), kind=kLoop, calls=%fused_computation.7 | loop fusion | flops 4194304 | bytes 4204544 | tf_op jit(solution)/shard_map/convert_element_type | solution.py:20
  20.9 6.0 %gather_fusion = bf16[1024,2048]{1,0:T(8,128)(2,1)} fusion(bf16[512,2048]{1,0:T(8,128)(2,1)S(1)} %fusion.2, s32[1024]{0:T(1024)S(1)} %fusion.53), kind=kCustom, calls=%fused_computation | custom fusion | bytes 8392704 | tf_op jit(solution)/shard_map/jit(_take)/gather | solution.py:170
  27.0 1.6 dynamic-slice_select_fusion
  28.6 32.9 %all_to_all.24 = bf16[8,128,512]{2,1,0:T(8,128)(2,1)} all-to-all(bf16[8,128,512]{2,1,0:T(8,128)(2,1)S(1)} %bitcast.92), channel_id=1, replica_groups=mesh['ep'=8,'tp'=4] {'ep'}, dimensions={0} | all-to-all | bytes 2097152 | tf_op jit(solution)/shard_map/all_to_all | solution.py:173
  61.6 33.6 %all-gather.2.cloned.1.call-done = bf16[1024,2048]{1,0:T(8,128)(2,1)} async-done(((bf16[1024,512]{1,0:T(8,128)(2,1)}), bf16[1024,2048]{1,0:T(8,128)(2,1)}) %all-gather.2.cloned.1.call-update) | async-done | bytes 4194320 | tf_op jit(solution)/shard_map/all_gather | solution.py:174
  95.2 4.5 %fusion.16 = f32[1024,256]{1,0:T(8,128)} fusion(bf16[1024,2048]{1,0:T(8,128)(2,1)} %all-gather.2.cloned.1.call-done, bf16[1,2048,256]{2,1,0:T(8,128)(2,1)S(1)} %copy-done.11), kind=kOutput, calls=%fused_computation.33 | convolution fusion | flops 1073741824 | bytes 6291456 | tf_op jit(solution)/shard_map/dot_general | solution.py:177
  99.8 8.8 %convolution_convert_fusion = bf16[1024,2048]{1,0:T(8,128)(2,1)} fusion(bf16[1024,2048]{1,0:T(8,128)(2,1)} %all-gather.2.cloned.1.call-done, bf16[1,256,2048]{2,1,0:T(8,128)(2,1)S(1)} %copy-done, bf16[1,2048,256]{2,1,0:T(8,128)(2,1)S(1)} %copy-done.12, f32[1024,256]{1,0:T(8,128)} %fusion.16), kind=kOutput, calls=%fused_computation.8 | convolution fusion | flops 2151153664 | bytes 11534336 | tf_op jit(solution)/shard_map/dot_general | solution.py:180
  108.6 0.6 copy-done.7
  109.6 0.3 fusion.37
  110.2 26.2 %all_gather.10 = bf16[1024,64]{0,1:T(8,128)(2,1)S(1)} all-gather(bf16[128,64]{0,1:T(8,128)(2,1)S(1)} %bitcast.99), channel_id=1, replica_groups=mesh['ep'=8,'tp'=4] {'ep'}, dimensions={0}, use_global_device_ids=true | all-gather | bytes 147456 | tf_op jit(solution)/shard_map/all_gather | solution.py:138
  136.4 0.2 fusion.9
  136.7 31.4 %all_gather.9 = bf16[1024,256]{1,0:T(8,128)(2,1)S(1)} all-gather(bf16[128,256]{1,0:T(8,128)(2,1)S(1)} %copy-done.6), channel_id=1, replica_groups=mesh['ep'=8,'tp'=4] {'ep'}, dimensions={0}, use_global_device_ids=true | all-gather | bytes 589824 | tf_op jit(solution)/shard_map/all_gather | solution.py:137
  168.1 0.2 fusion.10
  168.3 0.5 convolution_convert_fusion.3
  168.8 0.3 fusion.34
  169.1 0.4 fusion.59
  169.6 4.3 %all-to-all-start.1 = ((bf16[8,128,512]{2,1,0:T(8,128)(2,1)}), bf16[8,128,512]{2,1,0:T(8,128)(2,1)S(1)}, u32[]{:S(2)}, u32[]{:S(2)}) async-start(bf16[8,128,512]{2,1,0:T(8,128)(2,1)} %bitcast.93), calls=%async_computation.3 | async-start | bytes 2097152 | tf_op jit(solution)/shard_map/all_to_all | solution.py:184
  173.9 0.2 reduce-scatter.3.cloned.1.call-start
  174.2 0.3 fusion.23
  174.5 1.5 convolution_convert_fusion.2
  176.1 0.4 fusion.8
  176.5 1.2 convolution_convert_fusion.1
  178.4 12.0 %all-to-all-done.1 = bf16[8,128,512]{2,1,0:T(8,128)(2,1)S(1)} async-done(((bf16[8,128,512]{2,1,0:T(8,128)(2,1)}), bf16[8,128,512]{2,1,0:T(8,128)(2,1)S(1)}, u32[]{:S(2)}, u32[]{:S(2)}) %all-to-all-start.1) | async-done | bytes 1048608 | tf_op jit(solution)/shard_map/all_to_all | solution.py:184
  190.3 4.0 %gather_fusion.1 = bf16[1024,512]{1,0:T(8,128)(2,1)S(1)} fusion(bf16[1024,512]{1,0:T(8,128)(2,1)S(1)} %bitcast.90, s32[1024]{0:T(1024)S(1)} %broadcast_clamp_fusion), kind=kCustom, calls=%fused_computation.1 | custom fusion | bytes 2101248 | tf_op jit(solution)/shard_map/jit(_take)/gather | solution.py:186
  194.3 0.4 gather.12
  194.7 5.2 %multiply_reduce_fusion = bf16[512,512]{1,0:T(8,128)(2,1)} fusion(bf16[512,2,512]{2,1,0:T(2,128)(2,1)S(1)} %gather.12, pred[512,2]{1,0:T(8,128)(4,1)S(1)} %copy.43, f32[512,2]{1,0:T(8,128)S(1)} %copy.45), kind=kLoop, calls=%fused_computation.10 | loop fusion | flops 1835008 | bytes 1577984 | tf_op jit(solution)/shard_map/reduce_sum | solution.py:190
  (75 shorter events, 2.5 us)
Async XLA Ops:
  7.2 92.6 %copy-start = (bf16[1,256,2048]{2,1,0:T(8,128)(2,1)S(1)}, bf16[1,256,2048]{2,1,0:T(8,128)(2,1)}, u32[]{:S(2)}) copy-start(bf16[1,256,2048]{2,1,0:T(8,128)(2,1)} %param.33) | copy-start | bytes 3145732
  7.2 88.1 %all-gather.2.cloned.1.call-start = ((), (), s32[]{:S(2)}) async-start(), calls=%async_computation.5 | async-start | bytes 5242880 | tf_op jit(solution)/shard_map/all_gather | solution.py:174
  27.0 68.3 %copy-start.11 = (bf16[1,2048,256]{2,1,0:T(8,128)(2,1)S(1)}, bf16[1,2048,256]{2,1,0:T(8,128)(2,1)}, u32[]{:S(2)}) copy-start(bf16[1,2048,256]{2,1,0:T(8,128)(2,1)} %param.31) | copy-start | bytes 3145732
  61.6 38.2 %copy-start.12 = (bf16[1,2048,256]{2,1,0:T(8,128)(2,1)S(1)}, bf16[1,2048,256]{2,1,0:T(8,128)(2,1)}, u32[]{:S(2)}) copy-start(bf16[1,2048,256]{2,1,0:T(8,128)(2,1)} %param.32) | copy-start | bytes 3145732
  61.6 108.0 %reduce-scatter.5.cloned.1.call-start = ((), (), s32[]{:S(2)}) async-start(), calls=%async_computation.6 | async-start | bytes 5242880 | tf_op jit(solution)/shard_map/reduce_scatter | solution.py:181
  108.6 0.7 copy-start.7
  108.6 0.9 copy-start.2
  108.6 1.0 copy-start.5
  108.6 1.0 copy-start.9
  108.6 27.9 %copy-start.4 = (bf16[512,256]{1,0:T(8,128)(2,1)S(1)}, bf16[512,256]{1,0:T(8,128)(2,1)}, u32[]{:S(2)}) copy-start(bf16[512,256]{1,0:T(8,128)(2,1)} %param.22) | copy-start | bytes 786436
  108.6 28.1 %copy-start.6 = (bf16[128,256]{1,0:T(8,128)(2,1)S(1)}, bf16[128,256]{1,0:T(8,128)(2,1)}, u32[]{:S(2)}) copy-start(bf16[128,256]{1,0:T(8,128)(2,1)} %param.18) | copy-start | bytes 196612
  108.6 59.7 %copy-start.13 = (bf16[256,256]{1,0:T(8,128)(2,1)S(1)}, bf16[256,256]{1,0:T(8,128)(2,1)}, u32[]{:S(2)}) copy-start(bf16[256,256]{1,0:T(8,128)(2,1)} %param.24) | copy-start | bytes 393220
  108.6 59.7 %copy-start.15 = (f32[256]{0:T(256)S(1)}, f32[256]{0:T(256)}, u32[]{:S(2)}) copy-start(f32[256]{0:T(256)} %param.21) | copy-start | bytes 3076
  168.1 1.1 copy-start.1
  168.3 6.2 %copy-start.14 = (bf16[256,256]{1,0:T(8,128)(2,1)S(1)}, bf16[256,256]{1,0:T(8,128)(2,1)}, u32[]{:S(2)}) copy-start(bf16[256,256]{1,0:T(8,128)(2,1)} %param.25) | copy-start | bytes 393220
  169.6 8.4 %copy-start.8 = (s32[512,2]{0,1:T(2,128)S(1)}, s32[512,2]{0,1:T(2,128)}, u32[]{:S(2)}) copy-start(s32[512,2]{0,1:T(2,128)} %param.29) | copy-start | bytes 12292
  169.6 8.6 %copy-start.10 = (f32[512,2]{0,1:T(2,128)S(1)}, f32[512,2]{0,1:T(2,128)}, u32[]{:S(2)}) copy-start(f32[512,2]{0,1:T(2,128)} %param.30) | copy-start | bytes 12292
  169.6 20.7 %all-to-all-start.1 = ((bf16[8,128,512]{2,1,0:T(8,128)(2,1)}), bf16[8,128,512]{2,1,0:T(8,128)(2,1)S(1)}, u32[]{:S(2)}, u32[]{:S(2)}) async-start(bf16[8,128,512]{2,1,0:T(8,128)(2,1)} %bitcast.93), calls=%async_computation.3 | async-start | bytes 2097152 | tf_op jit(solution)/shard_map/all_to_all | solution.py:184
  173.9 26.0 %reduce-scatter.3.cloned.1.call-start = ((), (), s32[]{:S(2)}) async-start(), calls=%async_computation.4 | async-start | bytes 655360 | tf_op jit(solution)/shard_map/reduce_scatter | solution.py:145
  174.2 2.3 %copy-start.3 = (bf16[256,2048]{1,0:T(8,128)(2,1)S(1)}, bf16[256,2048]{1,0:T(8,128)(2,1)}, u32[]{:S(2)}) copy-start(bf16[256,2048]{1,0:T(8,128)(2,1)} %param.26) | copy-start | bytes 3145732
Sparse Core Ops, SparseCore 0:
  61.7 33.4 all-gather.1
  108.8 44.3 reduce-scatter.4
  177.8 22.1 reduce-scatter.2
where the time goes:
time: 207 us; the launch traced here: 206 us
  blocking collectives  90.5 us (44%)
  waiting for transfers between devices  45.7 us (22%)
  local copies, waits for them, and re-layouts  18.2 us (9%)
  matrix products  18.1 us (9%)
  other arithmetic  15.2 us (7%)
  between operations  14.2 us (7%)
  starting transfers between devices  4.65 us (2%)
    all_gather x1, waiting for transfers between devices, expert_half(): member = lax.all_gather(arrived, 'tp', axis=1, tiled=True)  33.6 us
    all_to_all x1, blocking collectives, expert_half(): lax.all_to_all(own_cols, 'ep', split_axis=0, concat_axis=0, tiled=True)  32.9 us
    all_gather x1, blocking collectives, mixer_half(): lax.all_gather(key_latent, 'ep', axis=0, tiled=True)  31.4 us
    all_gather x1, blocking collectives, mixer_half(): lax.all_gather(key_rot, 'ep', axis=0, tiled=True)  26.2 us
    all_to_all x1, waiting for transfers between devices, expert_half(): lax.all_to_all(shared, 'ep', split_axis=0, concat_axis=0, tiled=True)  12 us
    dot_general x1, matrix products, expert_half(): jnp.dot(hidden, w_down[0], preferred_element_type=jnp.float32)  8.8 us
    gather x1, local copies, waits for them, and re-layouts, expert_half(): outgoing = jnp.take(normed, source_row, axis=0)  6.02 us
    reduce_sum x1, other arithmetic, expert_half(): combined = jnp.sum(picked * route_weight[:, :, None], axis=1)  5.21 us
  transfers between devices with their start and end apart: 4, of which 2 were waited for; matrix products, arithmetic and copies ran while one was open for 8% of the time, Pallas kernels for 0%

commit v1 on v0

--- a/solution.py
+++ b/solution.py
@@ -171,7 +171,12 @@
     share_cols = outgoing.shape[1] // lax.axis_size("tp")
     own_cols = lax.dynamic_slice_in_dim(outgoing, lax.axis_index("tp") * share_cols, share_cols, 1)
     arrived = lax.all_to_all(own_cols, "ep", split_axis=0, concat_axis=0, tiled=True)
-    member = lax.all_gather(arrived, "tp", axis=1, tiled=True)
+    ring = [arrived]
+    for hop in range(3):
+        ring.append(lax.ppermute(ring[-1], "tp", [(dev, (dev + 1) % 4) for dev in range(4)]))
+    member = jnp.roll(
+        jnp.concatenate(ring[::-1], axis=1), (lax.axis_index("tp") + 1) * ring[0].shape[1], axis=1
+    )
     gate_rows = w_gate[0]
     up_rows = w_up[0]
     gate_act = jnp.dot(member, gate_rows, preferred_element_type=jnp.float32)

time: 207 us -> 224 us (1.082)
  waiting for transfers between devices: 45.7 us -> 55.8 us
  local copies, waits for them, and re-layouts: 18.2 us -> 26.8 us
    ppermute x0 -> x3, waiting for transfers between devices: none -> 43.1 us  [expert_half(): lax.ppermute(ring[-1], 'tp', [(dev, (dev + 1) % 4) for dev in range(4)])]
    all_gather x1 -> x0, waiting for transfers between devices: 33.6 us -> none  [expert_half(): member = lax.all_gather(arrived, 'tp', axis=1, tiled=True)]
    unnamed x34 -> x39, local copies, waits for them, and re-layouts: 1.93 us -> 10.3 us
    dot_general x1, matrix products: 4.51 us -> 1.26 us  [expert_half(): up_act = jnp.dot(member, up_rows, preferred_element_type=jnp.float32)]
  transfers between devices with their start and end apart: 4 -> 6, of which waited for: 2 -> 5; matrix products, arithmetic and copies ran while one was open for 8% -> 8% of each run, Pallas kernels for 0% -> 0%
where the time goes in v1:
time: 224 us; the launch traced here: 223 us
  blocking collectives  90.9 us (41%)
  waiting for transfers between devices  55.8 us (25%)
  local copies, waits for them, and re-layouts  26.8 us (12%)
  matrix products  16.2 us (7%)
  other arithmetic  15.1 us (7%)
  between operations  14.6 us (7%)
  starting transfers between devices  3.84 us (2%)
    ppermute x3, waiting for transfers between devices, expert_half(): lax.ppermute(ring[-1], 'tp', [(dev, (dev + 1) % 4) for dev in range(4)])  43.1 us
    all_to_all x1, blocking collectives, expert_half(): lax.all_to_all(own_cols, 'ep', split_axis=0, concat_axis=0, tiled=True)  32.8 us
    all_gather x1, blocking collectives, mixer_half(): lax.all_gather(key_latent, 'ep', axis=0, tiled=True)  31.9 us
    all_gather x1, blocking collectives, mixer_half(): lax.all_gather(key_rot, 'ep', axis=0, tiled=True)  26.1 us
    all_to_all x1, waiting for transfers between devices, expert_half(): lax.all_to_all(shared, 'ep', split_axis=0, concat_axis=0, tiled=True)  10.7 us
    unnamed x39, local copies, waits for them, and re-layouts  10.3 us
    dot_general x1, matrix products, expert_half(): jnp.dot(hidden, w_down[0], preferred_element_type=jnp.float32)  8.94 us
    gather x1, local copies, waits for them, and re-layouts, expert_half(): outgoing = jnp.take(normed, source_row, axis=0)  6.02 us
  transfers between devices with their start and end apart: 6, of which 5 were waited for; matrix products, arithmetic and copies ran while one was open for 8% of the time, Pallas kernels for 0%

profile of v1, /device:TPU:0, one launch (start us, length us, event | category | flops | bytes accessed | tf_op | source)
XLA Modules:
  0.0 223.2 jit_solution(12602436825409407142)
XLA Ops:
  7.2 0.9 copy.40
  8.5 0.7 broadcast_multiply_fusion.2
  9.2 2.3 %reduce-window.6 = s32[8,8,128]{2,1,0:T(8,128)S(1)} reduce-window(s32[8,8,128]{2,1,0:T(8,128)S(1)} %fusion.47, s32[]{:T(128)} %constant.125.clone.1), window={size=1x1x128 pad=0_0x0_0x127_0}, to_apply=%region_5.6 | reduce-window | flops 1040384 | bytes 65540 | tf_op jit(solution)/shard_map/reduce-window
  12.4 4.3 %scatter_custom_fusion = s32[1024]{0:T(1024)S(1)} fusion(s32[1024]{0:T(1024)S(1)} %bitcast.104, s32[1024]{0:T(1024)S(1)} %add_select_fusion, s32[]{:T(128)} %constant.125.clone.1), kind=kCustom, calls=%fused_computation.100 | custom fusion | bytes 4100 | tf_op jit(solution)/shard_map/scatter | solution.py:168
  16.7 2.1 fusion
  18.8 2.1 fusion.2
  20.9 6.0 %gather_fusion = bf16[1024,2048]{1,0:T(8,128)(2,1)} fusion(bf16[512,2048]{1,0:T(8,128)(2,1)S(1)} %fusion.2, s32[1024]{0:T(1024)S(1)} %fusion.57), kind=kCustom, calls=%fused_computation | custom fusion | bytes 8392704 | tf_op jit(solution)/shard_map/jit(_take)/gather | solution.py:170
  27.0 1.5 dynamic-slice_select_fusion
  28.5 32.8 %all_to_all.24 = bf16[8,128,512]{2,1,0:T(8,128)(2,1)S(1)} all-to-all(bf16[8,128,512]{2,1,0:T(8,128)(2,1)S(1)} %bitcast.95), channel_id=1, replica_groups=mesh['ep'=8,'tp'=4] {'ep'}, dimensions={0} | all-to-all | bytes 2097152 | tf_op jit(solution)/shard_map/all_to_all | solution.py:173
  61.4 14.2 %collective-permute-done = bf16[1024,512]{1,0:T(8,128)(2,1)S(1)} collective-permute-done((bf16[1024,512]{1,0:T(8,128)(2,1)S(1)}, bf16[1024,512]{1,0:T(8,128)(2,1)S(1)}, u32[]{:S(2)}, u32[]{:S(2)}) %collective-permute-start) | collective-permute-done | bytes 1048608 | tf_op jit(solution)/shard_map/ppermute | solution.py:176
  75.6 14.3 %collective-permute-done.1 = bf16[1024,512]{1,0:T(8,128)(2,1)} collective-permute-done((bf16[1024,512]{1,0:T(8,128)(2,1)S(1)}, bf16[1024,512]{1,0:T(8,128)(2,1)}, u32[]{:S(2)}, u32[]{:S(2)}) %collective-permute-start.1) | collective-permute-done | bytes 1048608 | tf_op jit(solution)/shard_map/ppermute | solution.py:176
  89.9 14.5 %collective-permute-done.2 = bf16[1024,512]{1,0:T(8,128)(2,1)} collective-permute-done((bf16[1024,512]{1,0:T(8,128)(2,1)}, bf16[1024,512]{1,0:T(8,128)(2,1)}, u32[]{:S(2)}, u32[]{:S(2)}) %collective-permute-start.2) | collective-permute-done | bytes 1048608 | tf_op jit(solution)/shard_map/ppermute | solution.py:176
  104.5 1.4 constant_dynamic-update-slice_fusion.7
  105.8 1.4 constant_dynamic-update-slice_fusion.6
  107.5 1.4 constant_dynamic-update-slice_fusion.3
  108.9 1.4 constant_dynamic-update-slice_fusion.2
  110.6 3.2 %copy-done.5 = bf16[1024,4096]{1,0:T(8,128)(2,1)} copy-done((bf16[1024,4096]{1,0:T(8,128)(2,1)}, bf16[1024,4096]{1,0:T(8,128)(2,1)S(1)}, u32[]{:S(2)}) %copy-start.5) | copy-done | bytes 8388632
  113.9 1.3 fusion.3
  115.2 8.9 %convolution_convert_fusion = bf16[1024,2048]{1,0:T(8,128)(2,1)} fusion(bf16[1,256,2048]{2,1,0:T(8,128)(2,1)S(1)} %copy-done, f32[1024,256]{1,0:T(8,128)S(1)} %fusion.3, bf16[1024,4096]{1,0:T(8,128)(2,1)} %copy-done.5, s32[]{:T(128)S(6)} %select_n.79, bf16[1,2048,256]{2,1,0:T(8,128)(2,1)} %param.31), kind=kOutput, calls=%fused_computation.8 | convolution fusion | flops 2151153664 | bytes 11534340 | tf_op jit(solution)/shard_map/dot_general | solution.py:185
  125.1 26.1 %all_gather.7 = bf16[1024,64]{0,1:T(8,128)(2,1)S(1)} all-gather(bf16[128,64]{0,1:T(8,128)(2,1)S(1)} %bitcast.102), channel_id=1, replica_groups=mesh['ep'=8,'tp'=4] {'ep'}, dimensions={0}, use_global_device_ids=true | all-gather | bytes 147456 | tf_op jit(solution)/shard_map/all_gather | solution.py:138
  151.4 31.9 %all_gather.6 = bf16[1024,256]{1,0:T(8,128)(2,1)S(1)} all-gather(bf16[128,256]{1,0:T(8,128)(2,1)S(1)} %copy-done.6), channel_id=1, replica_groups=mesh['ep'=8,'tp'=4] {'ep'}, dimensions={0}, use_global_device_ids=true | all-gather | bytes 589824 | tf_op jit(solution)/shard_map/all_gather | solution.py:137
  183.6 0.5 convolution_convert_fusion.3
  184.4 0.4 fusion.66
  184.9 3.6 %all-to-all-start.1 = ((bf16[8,128,512]{2,1,0:T(8,128)(2,1)}), bf16[8,128,512]{2,1,0:T(8,128)(2,1)S(1)}, u32[]{:S(2)}, u32[]{:S(2)}) async-start(bf16[8,128,512]{2,1,0:T(8,128)(2,1)} %bitcast.96), calls=%async_computation.3 | async-start | bytes 2097152 | tf_op jit(solution)/shard_map/all_to_all | solution.py:189
  189.0 1.5 convolution_convert_fusion.2
  190.5 0.4 fusion.11
  190.9 2.4 %convolution_convert_fusion.1 = bf16[128,2048]{1,0:T(8,128)(2,1)} fusion(bf16[128,256]{0,1:T(8,128)(2,1)S(1)} %bitcast.101, bf16[256,2048]{1,0:T(8,128)(2,1)} %param.26), kind=kOutput, calls=%fused_computation.13 | convolution fusion | flops 134479872 | bytes 1638400 | tf_op jit(solution)/shard_map/dot_general | solution.py:146
  194.1 10.7 %all-to-all-done.1 = bf16[8,128,512]{2,1,0:T(8,128)(2,1)S(1)} async-done(((bf16[8,128,512]{2,1,0:T(8,128)(2,1)}), bf16[8,128,512]{2,1,0:T(8,128)(2,1)S(1)}, u32[]{:S(2)}, u32[]{:S(2)}) %all-to-all-start.1) | async-done | bytes 1048608 | tf_op jit(solution)/shard_map/all_to_all | solution.py:189
  204.7 4.0 %gather_fusion.1 = bf16[1024,512]{1,0:T(8,128)(2,1)S(1)} fusion(bf16[1024,512]{1,0:T(8,128)(2,1)S(1)} %bitcast.91, s32[1024]{0:T(1024)S(1)} %broadcast_clamp_fusion), kind=kCustom, calls=%fused_computation.1 | custom fusion | bytes 2101248 | tf_op jit(solution)/shard_map/jit(_take)/gather | solution.py:191
  208.7 0.4 gather.12
  209.2 5.2 %multiply_reduce_fusion = bf16[512,512]{1,0:T(8,128)(2,1)} fusion(bf16[512,2,512]{2,1,0:T(2,128)(2,1)S(1)} %gather.12, pred[512,2]{1,0:T(8,128)(4,1)S(1)} %copy.43, f32[512,2]{1,0:T(8,128)S(1)} %copy.45), kind=kLoop, calls=%fused_computation.14 | loop fusion | flops 1835008 | bytes 1577984 | tf_op jit(solution)/shard_map/reduce_sum | solution.py:195
  214.4 2.0 reduce-scatter.3.cloned.1.call-done
  (84 shorter events, 4.7 us)
Async XLA Ops:
  7.2 108.0 %copy-start = (bf16[1,256,2048]{2,1,0:T(8,128)(2,1)S(1)}, bf16[1,256,2048]{2,1,0:T(8,128)(2,1)}, u32[]{:S(2)}) copy-start(bf16[1,256,2048]{2,1,0:T(8,128)(2,1)} %param.33) | copy-start | bytes 3145732
  7.2 177.7 %reduce-scatter.5.cloned.1.call-start = ((), (), s32[]{:S(2)}) async-start(), calls=%async_computation.5 | async-start | bytes 5242880 | tf_op jit(solution)/shard_map/reduce_scatter | solution.py:186
  61.4 14.2 %collective-permute-start = (bf16[1024,512]{1,0:T(8,128)(2,1)S(1)}, bf16[1024,512]{1,0:T(8,128)(2,1)S(1)}, u32[]{:S(2)}, u32[]{:S(2)}) collective-permute-start(bf16[1024,512]{1,0:T(8,128)(2,1)S(1)} %bitcast.92), channel_id=1, source_target_pairs={{0,1},{1,2},{2,3},{3,0},{4,5},{5,6},{6,7},{7,4},{8,9},{9,10},{10,1... | collective-permute-start | bytes 3145736 | tf_op jit(solution)/shard_map/ppermute | solution.py:176
  75.6 14.3 %collective-permute-start.1 = (bf16[1024,512]{1,0:T(8,128)(2,1)S(1)}, bf16[1024,512]{1,0:T(8,128)(2,1)}, u32[]{:S(2)}, u32[]{:S(2)}) collective-permute-start(bf16[1024,512]{1,0:T(8,128)(2,1)S(1)} %collective-permute-done), channel_id=1, source_target_pairs={{0,1},{1,2},{2,3},{3,0},{4,5},{5,6},{6,7},{7,4},{8,9},{9,10},{10,1... | collective-permute-start | bytes 3145736 | tf_op jit(solution)/shard_map/ppermute | solution.py:176
  89.9 14.5 %collective-permute-start.2 = (bf16[1024,512]{1,0:T(8,128)(2,1)}, bf16[1024,512]{1,0:T(8,128)(2,1)}, u32[]{:S(2)}, u32[]{:S(2)}) collective-permute-start(bf16[1024,512]{1,0:T(8,128)(2,1)} %collective-permute-done.1), channel_id=1, source_target_pairs={{0,1},{1,2},{2,3},{3,0},{4,5},{5,6},{6,7},{7,4},{8,9},{9,10},{10,1... | collective-permute-start | bytes 3145736 | tf_op jit(solution)/shard_map/ppermute | solution.py:176
  89.9 24.0 %copy-start.11 = (bf16[1,2048,256]{2,1,0:T(8,128)(2,1)S(1)}, bf16[1,2048,256]{2,1,0:T(8,128)(2,1)}, u32[]{:S(2)}) copy-start(bf16[1,2048,256]{2,1,0:T(8,128)(2,1)} %param.32) | copy-start | bytes 3145732
  110.6 3.2 %copy-start.5 = (bf16[1024,4096]{1,0:T(8,128)(2,1)}, bf16[1024,4096]{1,0:T(8,128)(2,1)S(1)}, u32[]{:S(2)}) copy-start(bf16[1024,4096]{1,0:T(8,128)(2,1)S(1)} %constant_dynamic-update-slice_fusion) | copy-start | bytes 25165828
  115.2 9.1 %copy-start.7 = (bf16[128,64]{0,1:T(8,128)(2,1)S(1)}, bf16[128,64]{0,1:T(8,128)(2,1)}, u32[]{:S(2)}) copy-start(bf16[128,64]{0,1:T(8,128)(2,1)} %param.19) | copy-start | bytes 49156
  115.2 9.1 %copy-start.2 = (bf16[128,512]{1,0:T(8,128)(2,1)S(1)}, bf16[128,512]{1,0:T(8,128)(2,1)}, u32[]{:S(2)}) copy-start(bf16[128,512]{1,0:T(8,128)(2,1)} %param.17) | copy-start | bytes 393220
  115.2 9.2 %copy-start.4 = (bf16[512,128]{1,0:T(8,128)(2,1)S(1)}, bf16[512,128]{1,0:T(8,128)(2,1)}, u32[]{:S(2)}) copy-start(bf16[512,128]{1,0:T(8,128)(2,1)} %param.23) | copy-start | bytes 393220
  115.2 9.2 %copy-start.9 = (f32[512]{0:T(512)S(1)}, f32[512]{0:T(512)}, u32[]{:S(2)}) copy-start(f32[512]{0:T(512)} %param.20) | copy-start | bytes 6148
  115.2 36.0 %copy-start.3 = (bf16[512,256]{1,0:T(8,128)(2,1)S(1)}, bf16[512,256]{1,0:T(8,128)(2,1)}, u32[]{:S(2)}) copy-start(bf16[512,256]{1,0:T(8,128)(2,1)} %param.22) | copy-start | bytes 786436
  115.2 36.2 %copy-start.6 = (bf16[128,256]{1,0:T(8,128)(2,1)S(1)}, bf16[128,256]{1,0:T(8,128)(2,1)}, u32[]{:S(2)}) copy-start(bf16[128,256]{1,0:T(8,128)(2,1)} %param.18) | copy-start | bytes 196612
  115.2 68.4 %copy-start.12 = (bf16[256,256]{1,0:T(8,128)(2,1)S(1)}, bf16[256,256]{1,0:T(8,128)(2,1)}, u32[]{:S(2)}) copy-start(bf16[256,256]{1,0:T(8,128)(2,1)} %param.24) | copy-start | bytes 393220
  115.2 68.4 %copy-start.14 = (f32[256]{0:T(256)S(1)}, f32[256]{0:T(256)}, u32[]{:S(2)}) copy-start(f32[256]{0:T(256)} %param.21) | copy-start | bytes 3076
  124.2 64.8 %copy-start.13 = (bf16[256,256]{1,0:T(8,128)(2,1)S(1)}, bf16[256,256]{1,0:T(8,128)(2,1)}, u32[]{:S(2)}) copy-start(bf16[256,256]{1,0:T(8,128)(2,1)} %param.25) | copy-start | bytes 393220
  124.2 69.4 %copy-start.8 = (s32[512,2]{0,1:T(2,128)S(1)}, s32[512,2]{0,1:T(2,128)}, u32[]{:S(2)}) copy-start(s32[512,2]{0,1:T(2,128)} %param.29) | copy-start | bytes 12292
  124.3 69.6 %copy-start.10 = (f32[512,2]{0,1:T(2,128)S(1)}, f32[512,2]{0,1:T(2,128)}, u32[]{:S(2)}) copy-start(f32[512,2]{0,1:T(2,128)} %param.30) | copy-start | bytes 12292
  183.4 1.0 copy-start.1
  184.9 19.9 %all-to-all-start.1 = ((bf16[8,128,512]{2,1,0:T(8,128)(2,1)}), bf16[8,128,512]{2,1,0:T(8,128)(2,1)S(1)}, u32[]{:S(2)}, u32[]{:S(2)}) async-start(bf16[8,128,512]{2,1,0:T(8,128)(2,1)} %bitcast.96), calls=%async_computation.3 | async-start | bytes 2097152 | tf_op jit(solution)/shard_map/all_to_all | solution.py:189
  188.4 28.0 %reduce-scatter.3.cloned.1.call-start = ((), (), s32[]{:S(2)}) async-start(), calls=%async_computation.4 | async-start | bytes 655360 | tf_op jit(solution)/shard_map/reduce_scatter | solution.py:145
Sparse Core Ops, SparseCore 0:
  124.3 43.4 reduce-scatter.4
  193.5 22.8 reduce-scatter.2
